TPU v7x, 32 devices: a whole 2x2x4 slice. The times are simulated.
32 devices in a mesh: ep: 16 (over z, y, x), tp: 2 (over core).
Axes of the slice: x: 2, y: 2, z: 4, core: 2. Of those that a mesh axis runs over, the one named last changes fastest.
Arguments:
- resid: bfloat16 [256, 2048], P('ep'), may hold values from -6 to 6
- proj_x: bfloat16 [256, 2048], P('ep', 'tp'), may hold values from -6 to 6
- proj_z: bfloat16 [256, 2048], P('ep', 'tp'), may hold values from -6 to 6
- proj_bc: bfloat16 [256, 2, 512], P('ep', None, 'tp'), may hold values from -6 to 6
- proj_dt: bfloat16 [256, 32], P('ep', 'tp'), may hold values from -6 to 6
- tail_x: bfloat16 [256, 3, 2048], P('ep', None, 'tp'), may hold values from -6 to 6
- tail_bc: bfloat16 [256, 3, 2, 512], P('ep', None, None, 'tp'), may hold values from -6 to 6
- taps_x: bfloat16 [4, 2048], P(None, 'tp'), may hold values from -3 to 3
- taps_bc: bfloat16 [4, 2, 512], P(None, None, 'tp'), may hold values from -3 to 3
- ssm_state: float32 [256, 32, 4096], P('ep', 'tp'), may hold values from -1.5 to 1.5
- dt_bias: float32 [32], P('tp'), may hold values from -4 to 0
- decay_log: float32 [32], P('tp'), may hold values from -1 to 2.5
- group_gain: float32 [2048], P('tp'), may hold values from 0.1 to 1.9
- out_proj: bfloat16 [2048, 2048], P('tp', 'ep'), may hold values from -0.125 to 0.125
- ffn_gain: float32 [2048], replicated, may hold values from 0.1 to 1.9
- dense_gate: bfloat16 [2048, 4096], P(None, ('ep', 'tp')), may hold values from -0.125 to 0.125
- dense_up: bfloat16 [2048, 4096], P(None, ('ep', 'tp')), may hold values from -0.125 to 0.125
- dense_down: bfloat16 [4096, 2048], P(('ep', 'tp')), may hold values from -0.09375 to 0.09375
- branch_gate: bfloat16 [2048], replicated, may hold values from -0.125 to 0.125
- group_weights: float32 [256, 4], replicated, may hold values from 0.2 to 1
- expert_ids: int32 [256, 6], replicated, may hold values from 0 to 15, all different within a row; in each aligned block of 16 rows (0 to 15, 16 to 31, ...) at most 7 rows name the same one
- expert_weights: float32 [256, 6], replicated, may hold values from 0.1 to 1
- exp_gate: bfloat16 [16, 2048, 512], P('ep', None, 'tp'), may hold values from -0.125 to 0.125
- exp_up: bfloat16 [16, 2048, 512], P('ep', None, 'tp'), may hold values from -0.125 to 0.125
- exp_down: bfloat16 [16, 512, 2048], P('ep', 'tp'), may hold values from -0.25 to 0.25
Outputs:
- out: bfloat16 [256, 2048], P(('ep', 'tp'))
- new_state: float32 [256, 32, 4096], P('ep', 'tp')
Inputs may be any that keep to these rules, and one draw needn't show every extreme that they name: `expert_ids`: each row names 6 different experts. In the rows of one index of ep (aligned blocks of 16 rows) no expert is named more than 7 times, a bound that some block reaches.
All inputs are finite; a program needn't handle non-finite values.
Results may differ from a plain program's by a relative error of at most 0.013.
Values may be sent and summed in bfloat16 or wider, within the bound.
A program may use at most 128 MiB of HBM per device.

v0:
```python
import jax
import jax.numpy as jnp
from jax import lax
from jax.sharding import PartitionSpec as P

HEAD_P = 64
NSTATE = 64
GROUPS = 4
TOPK = 6
HPG = 4
EPSILON = 1e-06


def state_update(
    proj_x,
    proj_z,
    proj_bc,
    proj_dt,
    tail_x,
    tail_bc,
    taps_x,
    taps_bc,
    ssm_state,
    dt_bias,
    decay_log,
    group_gain,
):
    window_x = jnp.concatenate([tail_x, proj_x[:, None]], axis=1).astype(jnp.float32)
    conv_x = jax.nn.silu(jnp.sum(window_x * taps_x.astype(jnp.float32)[None], axis=1))
    window_bc = jnp.concatenate([tail_bc, proj_bc[:, None]], axis=1).astype(jnp.float32)
    conv_bc = jax.nn.silu(jnp.sum(window_bc * taps_bc.astype(jnp.float32)[None], axis=1))
    count = proj_x.shape[0]
    heads = proj_dt.shape[1]
    x_heads = conv_x.reshape(count, heads, HEAD_P)
    grouped_bc = conv_bc.reshape(count, 2, heads // HPG, NSTATE)
    input_heads = jnp.repeat(grouped_bc[:, 0], HPG, axis=1)
    read_heads = jnp.repeat(grouped_bc[:, 1], HPG, axis=1)
    step_size = jax.nn.softplus(proj_dt.astype(jnp.float32) + dt_bias)
    decay = jnp.exp(-step_size * jnp.exp(decay_log))
    state = ssm_state.reshape(count, heads, HEAD_P, NSTATE)
    fresh = (step_size[:, :, None] * x_heads)[:, :, :, None] * input_heads[:, :, None, :]
    new_state = decay[:, :, None, None] * state + fresh
    readout = jnp.sum(new_state * read_heads[:, :, None, :], axis=-1)
    gated = readout.reshape(count, heads * HEAD_P) * jax.nn.silu(proj_z.astype(jnp.float32))
    grouped = gated.reshape(count, heads // HPG, HPG * HEAD_P)
    grouped = grouped * lax.rsqrt(jnp.mean(grouped * grouped, axis=-1, keepdims=True) + EPSILON)
    y_out = (grouped.reshape(count, heads * HEAD_P) * group_gain).astype(jnp.bfloat16)
    return (y_out, new_state.reshape(count, heads, HEAD_P * NSTATE))


def shards(
    resid,
    proj_x,
    proj_z,
    proj_bc,
    proj_dt,
    tail_x,
    tail_bc,
    taps_x,
    taps_bc,
    ssm_state,
    dt_bias,
    decay_log,
    group_gain,
    out_proj,
    ffn_gain,
    dense_gate,
    dense_up,
    dense_down,
    branch_gate,
    group_weights,
    expert_ids,
    expert_weights,
    exp_gate,
    exp_up,
    exp_down,
):
    y_out, new_state = state_update(
        proj_x,
        proj_z,
        proj_bc,
        proj_dt,
        tail_x,
        tail_bc,
        taps_x,
        taps_bc,
        ssm_state,
        dt_bias,
        decay_log,
        group_gain,
    )
    partial_value = jnp.dot(
        lax.all_gather(y_out, "ep", axis=0, tiled=True),
        out_proj,
        preferred_element_type=jnp.float32,
    )
    partial_value = lax.all_to_all(
        partial_value.astype(jnp.bfloat16), "ep", split_axis=0, concat_axis=1, tiled=True
    ).astype(partial_value.dtype)
    mixed = lax.psum(partial_value.astype(jnp.bfloat16), "tp").astype(jnp.float32)
    resid_new = (resid.astype(jnp.float32) + mixed).astype(jnp.bfloat16)
    widened = resid_new.astype(jnp.float32)
    normed = (
        widened
        * lax.rsqrt(jnp.mean(widened * widened, axis=-1, keepdims=True) + EPSILON)
        * ffn_gain
    ).astype(jnp.bfloat16)
    gathered = lax.all_gather(normed, "ep", axis=0, tiled=True)
    score = jnp.dot(gathered, branch_gate, preferred_element_type=jnp.float32)
    dense_pre = jnp.dot(gathered, dense_gate, preferred_element_type=jnp.float32)
    dense_lin = jnp.dot(gathered, dense_up, preferred_element_type=jnp.float32)
    dense_hidden = (jax.nn.sigmoid(score)[:, None] * jax.nn.silu(dense_pre) * dense_lin).astype(
        jnp.bfloat16
    )
    experts = lax.axis_size("ep")
    expert_own = lax.axis_index("ep")
    cores = lax.axis_size("tp")
    core_index = lax.axis_index("tp")
    batch = gathered.shape[0]
    rows_each = batch // experts
    half_rows = rows_each // cores
    pairs = rows_each * TOPK
    capacity = (pairs + experts - 1) // experts + 1
    group_size = experts // GROUPS
    levels = jnp.arange(1, capacity + 1, dtype=jnp.int32)
    pair_row = jnp.arange(pairs, dtype=jnp.int32) // TOPK
    pick = (jnp.arange(GROUPS, dtype=jnp.int32) == expert_own // group_size).astype(jnp.float32)
    coarse = jnp.sum(group_weights * pick[None], axis=1)
    pair_weight = (expert_weights * coarse[:, None]).reshape(experts, pairs)
    hits = (expert_ids.reshape(experts, pairs) == expert_own).astype(jnp.int32)
    ranks = jnp.cumsum(hits, axis=1, dtype=jnp.int32)
    select = hits[:, None, :] * (ranks[:, None, :] == levels[None, :, None]).astype(jnp.int32)
    local_row = jnp.sum(select * pair_row[None, None, :], axis=-1, dtype=jnp.int32)
    filled = jnp.sum(select, axis=-1, dtype=jnp.int32).reshape(-1)
    slot_weight = jnp.sum(select.astype(jnp.float32) * pair_weight[:, None, :], axis=-1).reshape(-1)
    row_index = (local_row + jnp.arange(experts, dtype=jnp.int32)[:, None] * rows_each).reshape(-1)
    slot_rows = jnp.take(gathered, row_index, axis=0)
    slot_pre = jnp.dot(slot_rows, exp_gate[0], preferred_element_type=jnp.float32)
    slot_lin = jnp.dot(slot_rows, exp_up[0], preferred_element_type=jnp.float32)
    slot_hidden = (slot_weight[:, None] * jax.nn.silu(slot_pre) * slot_lin).astype(jnp.bfloat16)
    placing = (jnp.arange(batch, dtype=jnp.int32)[:, None] == row_index[None, :]) & (
        filled[None, :] > 0
    )
    row_hidden = jnp.dot(
        placing.astype(jnp.bfloat16), slot_hidden, preferred_element_type=jnp.float32
    ).astype(jnp.bfloat16)
    joined = jnp.concatenate([dense_hidden, row_hidden], axis=1)
    down_all = jnp.concatenate([dense_down, exp_down[0]], axis=0)
    inner_width = joined.shape[1]
    ordered = (
        joined.reshape(experts, cores, half_rows, inner_width)
        .transpose(1, 0, 2, 3)
        .reshape(batch, inner_width)
    )
    halved = lax.psum_scatter(
        jnp.dot(ordered, down_all, preferred_element_type=jnp.float32).astype(jnp.bfloat16),
        "tp",
        scatter_dimension=0,
        tiled=True,
    ).astype(jnp.float32)
    branch = lax.psum_scatter(halved, "ep", scatter_dimension=0, tiled=True)
    own_rows = lax.dynamic_slice_in_dim(widened, core_index * half_rows, half_rows, 0)
    out = (own_rows + branch).astype(jnp.bfloat16)
    return (out, new_state)


def solution(mesh):
    return jax.shard_map(
        shards,
        mesh=mesh,
        in_specs=(
            P("ep", None),
            P("ep", "tp"),
            P("ep", "tp"),
            P("ep", None, "tp"),
            P("ep", "tp"),
            P("ep", None, "tp"),
            P("ep", None, None, "tp"),
            P(None, "tp"),
            P(None, None, "tp"),
            P("ep", "tp", None),
            P("tp"),
            P("tp"),
            P("tp"),
            P("tp", "ep"),
            P(),
            P(None, ("ep", "tp")),
            P(None, ("ep", "tp")),
            P(("ep", "tp"), None),
            P(),
            P(),
            P(),
            P(),
            P("ep", None, "tp"),
            P("ep", None, "tp"),
            P("ep", "tp", None),
        ),
        out_specs=(P(("ep", "tp"), None), P("ep", "tp", None)),
        check_vma=False,
    )
```

profile of v0, /device:TPU:0, one launch (start us, length us, event | category | flops | bytes accessed | tf_op | source)
XLA Modules:
  0.0 270.5 jit_solution(9776574114942145212)
XLA Ops:
  7.2 0.7 exp.39
  8.6 0.9 multiply_reduce_fusion.3
  10.4 0.9 multiply_reduce_fusion.1
  11.5 7.9 %reshape.179 = f32[16,16,64,64]{3,2,1,0:T(8,128)} reshape(f32[16,16,4096]{2,1,0:T(8,128)} %param.34) | data formatting | bytes 8388608 | tf_op jit(solution)/shard_map/reshape | solution.py:40
  19.7 8.5 %broadcast_multiply_fusion = (f32[16,16,64,64]{3,2,1,0:T(8,128)}, f32[16,16,64]{2,1,0:T(8,128)S(1)}) fusion(f32[16,16,64]{2,1,0:T(8,128)S(1)} %bitcast.44, f32[16,16,64]{2,1,0:T(8,128)S(1)} %multiply_multiply_fusion, f32[16,16,64]{2,1,0:T(8,128)S(1)} %bitcast.45, f32[16,16,64,64]{3,2,1,0:T(8,128)} %reshape.179, f32[16,16]{1,0:T(8,128)S(1)} %get-tuple-element.11), kind=kLoop, calls=%fused_computation.3 | loop fusion | flops 5226496 | bytes 8651776 | tf_op jit(solution)/shard_map/mul | solution.py:41
  28.7 45.3 %all_gather.6 = bf16[256,1024]{1,0:T(8,128)(2,1)S(1)} all-gather(bf16[16,1024]{1,0:T(8,128)(2,1)S(1)} %multiply_convert_fusion.1), channel_id=1, replica_groups=mesh['ep'=16,'tp'=2] {'ep'}, dimensions={0}, use_global_device_ids=true | all-gather | bytes 557056 | tf_op jit(solution)/shard_map/all_gather | solution.py:93
  74.0 0.9 convolution_convert_fusion.2
  74.9 3.5 %all-to-all-start = ((bf16[16,16,128]{2,1,0:T(8,128)(2,1)}), bf16[16,16,128]{2,1,0:T(8,128)(2,1)S(1)}, u32[]{:S(2)}, u32[]{:S(2)}) async-start(bf16[16,16,128]{2,1,0:T(8,128)(2,1)} %bitcast.6), calls=%async_computation | async-start | bytes 131072 | tf_op jit(solution)/shard_map/all_to_all | solution.py:97
  78.5 7.4 %all-to-all-done = bf16[16,16,128]{2,1,0:T(8,128)(2,1)S(1)} async-done(((bf16[16,16,128]{2,1,0:T(8,128)(2,1)}), bf16[16,16,128]{2,1,0:T(8,128)(2,1)S(1)}, u32[]{:S(2)}, u32[]{:S(2)}) %all-to-all-start) | async-done | bytes 65568 | tf_op jit(solution)/shard_map/all_to_all | solution.py:97
  86.7 14.5 %all-reduce.2.cloned.1.call-done = bf16[16,2048]{1,0:T(8,128)(2,1)} async-done(((bf16[16,2048]{1,0:T(8,128)(2,1)}), bf16[16,2048]{1,0:T(8,128)(2,1)}) %all-reduce.2.cloned.1.call-update) | async-done | bytes 65552 | tf_op jit(solution)/shard_map/psum | solution.py:100
  101.2 1.0 fusion.21
  102.1 1.6 multiply_convert_fusion
  106.0 54.8 %all-gather.2.cloned.1.call-done = bf16[256,2048]{1,0:T(8,128)(2,1)} async-done(((bf16[16,2048]{1,0:T(8,128)(2,1)}), bf16[256,2048]{1,0:T(8,128)(2,1)}) %all-gather.2.cloned.1.call-update) | async-done | bytes 1048592 | tf_op jit(solution)/shard_map/all_gather | solution.py:108
  160.8 1.6 fusion.36
  162.4 2.8 %gather_fusion = bf16[112,2048]{1,0:T(8,128)(2,1)S(1)} fusion(bf16[256,2048]{1,0:T(8,128)(2,1)} %all-gather.2.cloned.1.call-done, s32[1024]{0:T(1024)S(1)} %pad_clamp_fusion), kind=kCustom, calls=%fused_computation | custom fusion | bytes 917952 | tf_op jit(solution)/shard_map/jit(_take)/gather | solution.py:137
  165.3 1.6 fusion.7
  168.0 1.5 fusion.3
  169.7 3.0 %convolution_convert_fusion = bf16[256,2048]{1,0:T(8,128)(2,1)} fusion(bf16[256,384]{1,0:T(8,128)(2,1)S(1)} %bitcast.48, bf16[256,2048]{1,0:T(8,128)(2,1)} %bitcast.52, bf16[128,2048]{1,0:T(8,128)(2,1)} %param.42), kind=kOutput, calls=%fused_computation.4 | convolution fusion | flops 406323200 | bytes 2818048 | tf_op jit(solution)/shard_map/dot_general | solution.py:156
  172.8 7.3 %reduce-scatter.3.cloned.1.call-done = bf16[128,2048]{1,0:T(8,128)(2,1)} async-done(((bf16[256,2048]{1,0:T(8,128)(2,1)}), bf16[128,2048]{1,0:T(8,128)(2,1)}) %reduce-scatter.3.cloned.1.call-update) | async-done | bytes 524304 | tf_op jit(solution)/shard_map/reduce_scatter | solution.py:155
  180.2 2.2 convert_element_type.106
  182.4 7.9 %mul.284 = f32[16,16,4096]{2,1,0:T(8,128)} reshape(f32[16,16,64,64]{3,2,1,0:T(8,128)} %get-tuple-element.4) | data formatting | bytes 8388608 | tf_op jit(solution)/shard_map/mul | solution.py:41
  190.3 6.6 %multiply_add_fusion = f32[16,16,4096]{2,1,0:T(8,128)} fusion(f32[16,16,4096]{2,1,0:T(8,128)} %mul.284, f32[16,16,4096]{2,1,0:T(8,128)} %param.34, f32[16,16]{1,0:T(8,128)S(1)} %get-tuple-element.11), kind=kLoop, calls=%fused_computation.2 | loop fusion | flops 2097152 | bytes 12583936 | tf_op jit(solution)/shard_map/add | solution.py:42
  196.9 65.7 %reduce-scatter.5.cloned.1.call-done = f32[8,2048]{1,0:T(8,128)} async-done(((f32[128,2048]{1,0:T(8,128)}), f32[8,2048]{1,0:T(8,128)}) %reduce-scatter.5.cloned.1.call-update) | async-done | bytes 65552 | tf_op jit(solution)/shard_map/reduce_scatter | solution.py:161
  262.5 1.5 add_convert_fusion.1
  (89 shorter events, 6.5 us)
Async XLA Ops:
  7.2 159.7 %copy-start = (bf16[1,2048,256]{2,1,0:T(8,128)(2,1)S(1)}, bf16[1,2048,256]{2,1,0:T(8,128)(2,1)}, u32[]{:S(2)}) copy-start(bf16[1,2048,256]{2,1,0:T(8,128)(2,1)} %param.48) | copy-start | bytes 3145732
  11.5 7.9 %copy-start.12 = (bf16[16,16]{1,0:T(8,128)(2,1)S(1)}, bf16[16,16]{1,0:T(8,128)(2,1)}, u32[]{:S(2)}) copy-start(bf16[16,16]{1,0:T(8,128)(2,1)} %param.29) | copy-start | bytes 1540
  11.5 7.9 %copy-start.13 = (f32[16]{0:T(128)S(1)}, f32[16]{0:T(128)}, u32[]{:S(2)}) copy-start(f32[16]{0:T(128)} %param.35) | copy-start | bytes 196
  19.6 8.7 %copy-start.5 = (bf16[16,1024]{1,0:T(8,128)(2,1)S(1)}, bf16[16,1024]{1,0:T(8,128)(2,1)}, u32[]{:S(2)}) copy-start(bf16[16,1024]{1,0:T(8,128)(2,1)} %param.27) | copy-start | bytes 98308
  19.6 9.0 %copy-start.9 = (f32[1024]{0:T(1024)S(1)}, f32[1024]{0:T(1024)}, u32[]{:S(2)}) copy-start(f32[1024]{0:T(1024)} %param.37) | copy-start | bytes 12292
  19.6 54.4 %copy-start.3 = (bf16[1024,128]{1,0:T(8,128)(2,1)S(1)}, bf16[1024,128]{1,0:T(8,128)(2,1)}, u32[]{:S(2)}) copy-start(bf16[1024,128]{1,0:T(8,128)(2,1)} %param.38) | copy-start | bytes 786436
  19.6 67.0 %copy-start.7 = (s32[256,6]{0,1:T(8,128)S(1)}, s32[256,6]{0,1:T(8,128)}, u32[]{:S(2)}) copy-start(s32[256,6]{0,1:T(8,128)} %param.45) | copy-start | bytes 18436
  19.6 81.5 %copy-start.4 = (bf16[16,2048]{1,0:T(8,128)(2,1)S(1)}, bf16[16,2048]{1,0:T(8,128)(2,1)}, u32[]{:S(2)}) copy-start(bf16[16,2048]{1,0:T(8,128)(2,1)} %param.25) | copy-start | bytes 196612
  19.6 82.5 %copy-start.6 = (f32[2048]{0:T(1024)S(1)}, f32[2048]{0:T(1024)}, u32[]{:S(2)}) copy-start(f32[2048]{0:T(1024)} %param.39) | copy-start | bytes 24580
  19.7 85.3 %copy-start.11 = (f32[256,4]{0,1:T(4,128)S(1)}, f32[256,4]{0,1:T(4,128)}, u32[]{:S(2)}) copy-start(f32[256,4]{0,1:T(4,128)} %param.44) | copy-start | bytes 12292
  19.7 85.4 %copy-start.8 = (f32[256,6]{0,1:T(8,128)S(1)}, f32[256,6]{0,1:T(8,128)}, u32[]{:S(2)}) copy-start(f32[256,6]{0,1:T(8,128)} %param.46) | copy-start | bytes 18436
  19.7 86.2 %copy-start.10 = (bf16[2048]{0:T(1024)(128)(2,1)S(1)}, bf16[2048]{0:T(1024)(128)(2,1)}, u32[]{:S(2)}) copy-start(bf16[2048]{0:T(1024)(128)(2,1)} %param.43) | copy-start | bytes 12292
  74.9 11.0 %all-to-all-start = ((bf16[16,16,128]{2,1,0:T(8,128)(2,1)}), bf16[16,16,128]{2,1,0:T(8,128)(2,1)S(1)}, u32[]{:S(2)}, u32[]{:S(2)}) async-start(bf16[16,16,128]{2,1,0:T(8,128)(2,1)} %bitcast.6), calls=%async_computation | async-start | bytes 131072 | tf_op jit(solution)/shard_map/all_to_all | solution.py:97
  78.4 22.7 %all-reduce.2.cloned.1.call-start = ((), (), s32[]{:S(2)}) async-start(), calls=%async_computation.3 | async-start | bytes 131072 | tf_op jit(solution)/shard_map/psum | solution.py:100
  86.6 74.2 %all-gather.2.cloned.1.call-start = ((), (), s32[]{:S(2)}) async-start(), calls=%async_computation.4 | async-start | bytes 1114112 | tf_op jit(solution)/shard_map/all_gather | solution.py:108
  103.7 76.4 %reduce-scatter.3.cloned.1.call-start = ((), (), s32[]{:S(2)}) async-start(), calls=%async_computation.5 | async-start | bytes 1572864 | tf_op jit(solution)/shard_map/reduce_scatter | solution.py:155
  162.4 5.0 %copy-start.1 = (bf16[256,2048]{1,0:T(8,128)(2,1)S(1)}, bf16[256,2048]{1,0:T(8,128)(2,1)}, u32[]{:S(2)}) copy-start(bf16[256,2048]{1,0:T(8,128)(2,1)} %all-gather.2.cloned.1.call-done) | copy-start | bytes 3145732
  162.4 5.1 %copy-start.2 = (bf16[2048,128]{1,0:T(8,128)(2,1)S(1)}, bf16[2048,128]{1,0:T(8,128)(2,1)}, u32[]{:S(2)}) copy-start(bf16[2048,128]{1,0:T(8,128)(2,1)} %param.40) | copy-start | bytes 1572868
  172.8 89.7 %reduce-scatter.5.cloned.1.call-start = ((), (), s32[]{:S(2)}) async-start(), calls=%async_computation.6 | async-start | bytes 1114112 | tf_op jit(solution)/shard_map/reduce_scatter | solution.py:161
Sparse Core Ops, SparseCore 0:
  86.7 14.3 all-reduce.1
  104.5 56.2 all-gather.1
  172.9 7.2 reduce-scatter.2
  182.5 79.9 reduce-scatter.4
where the time goes:
time: 272 us; the launch traced here: 271 us
  waiting for transfers between devices  150 us (55%)
  blocking collectives  45.3 us (17%)
  other arithmetic  25.9 us (10%)
  local copies, waits for them, and re-layouts  21.8 us (8%)
  between operations  14.3 us (5%)
  matrix products  9.75 us (4%)
  starting transfers between devices  3.67 us (1%)
    reduce_scatter x1, waiting for transfers between devices, shards(): branch = lax.psum_scatter(halved, 'ep', scatter_dimension=0, tiled=True)  65.7 us
    all_gather x1, waiting for transfers between devices, shards(): gathered = lax.all_gather(normed, 'ep', axis=0, tiled=True)  54.8 us
    all_gather x1, blocking collectives, shards(): lax.all_gather(y_out, 'ep', axis=0, tiled=True)  45.3 us
    psum x1, waiting for transfers between devices, shards(): lax.psum(partial_value.astype(jnp.bfloat16), 'tp').astype(jnp.float32)  14.5 us
    mul x1, other arithmetic, state_update(): (step_size[:, :, None] * x_heads)[:, :, :, None]  8.51 us
    reshape x1, local copies, waits for them, and re-layouts, state_update(): state = ssm_state.reshape(count, heads, HEAD_P, NSTATE)  7.89 us
    mul x1, local copies, waits for them, and re-layouts, state_update(): (step_size[:, :, None] * x_heads)[:, :, :, None]  7.88 us
    all_to_all x1, waiting for transfers between devices, shards(): lax.all_to_all(partial_value.astype(jnp.bfloat16), 'ep', split_axis=0, co...  7.45 us
  transfers between devices with their start and end apart: 5, of which 5 were waited for; matrix products, arithmetic and copies ran while one was open for 6% of the time, Pallas kernels for 0%

commit v1 on v0

--- a/solution.py
+++ b/solution.py
@@ -9,6 +9,13 @@
 TOPK = 6
 HPG = 4
 EPSILON = 1e-06
+
+
+def swapped_in(x, name, along):
+    size = lax.axis_size(name)
+    tiles = jnp.stack([x for _ in range(size)])
+    tiles = lax.all_to_all(tiles, name, split_axis=0, concat_axis=0)
+    return jnp.concatenate(tiles, axis=along)
 
 
 def state_update(
@@ -90,9 +97,7 @@
         group_gain,
     )
     partial_value = jnp.dot(
-        lax.all_gather(y_out, "ep", axis=0, tiled=True),
-        out_proj,
-        preferred_element_type=jnp.float32,
+        swapped_in(y_out, "ep", 0), out_proj, preferred_element_type=jnp.float32
     )
     partial_value = lax.all_to_all(
         partial_value.astype(jnp.bfloat16), "ep", split_axis=0, concat_axis=1, tiled=True

time: 272 us -> 250 us (0.919)
  blocking collectives: 45.3 us -> 23.2 us
    all_gather x1 -> x0, blocking collectives: 45.3 us -> none  [shards(): lax.all_gather(y_out, 'ep', axis=0, tiled=True)]
    all_to_all x0 -> x1, blocking collectives: none -> 23.2 us  [swapped_in(): tiles = lax.all_to_all(tiles, name, split_axis=0, concat_axis=0)]
  transfers between devices with their start and end apart: 5 -> 5, of which waited for: 5 -> 5; matrix products, arithmetic and copies ran while one was open for 6% -> 7% of each run, Pallas kernels for 0% -> 0%
where the time goes in v1:
time: 250 us; the launch traced here: 249 us
  waiting for transfers between devices  150 us (60%)
  other arithmetic  25.8 us (10%)
  blocking collectives  23.2 us (9%)
  local copies, waits for them, and re-layouts  21.9 us (9%)
  between operations  14.2 us (6%)
  matrix products  9.75 us (4%)
  starting transfers between devices  4.12 us (2%)
    reduce_scatter x1, waiting for transfers between devices, shards(): branch = lax.psum_scatter(halved, 'ep', scatter_dimension=0, tiled=True)  65.8 us
    all_gather x1, waiting for transfers between devices, shards(): gathered = lax.all_gather(normed, 'ep', axis=0, tiled=True)  54.8 us
    all_to_all x1, blocking collectives, swapped_in(): tiles = lax.all_to_all(tiles, name, split_axis=0, concat_axis=0)  23.2 us
    psum x1, waiting for transfers between devices, shards(): lax.psum(partial_value.astype(jnp.bfloat16), 'tp').astype(jnp.float32)  14.6 us
    mul x1, other arithmetic, state_update(): (step_size[:, :, None] * x_heads)[:, :, :, None]  8.47 us
    reshape x1, local copies, waits for them, and re-layouts, state_update(): state = ssm_state.reshape(count, heads, HEAD_P, NSTATE)  7.89 us
    mul x1, local copies, waits for them, and re-layouts, state_update(): (step_size[:, :, None] * x_heads)[:, :, :, None]  7.88 us
    all_to_all x1, waiting for transfers between devices, shards(): lax.all_to_all(partial_value.astype(jnp.bfloat16), 'ep', split_axis=0, co...  7.48 us
  transfers between devices with their start and end apart: 5, of which 5 were waited for; matrix products, arithmetic and copies ran while one was open for 7% of the time, Pallas kernels for 0%

profile of v1, /device:TPU:0, one launch (start us, length us, event | category | flops | bytes accessed | tf_op | source)
XLA Modules:
  0.0 249.1 jit_solution(12635895204654175837)
XLA Ops:
  7.2 0.7 exp.39
  8.6 0.9 multiply_reduce_fusion.3
  10.4 0.9 multiply_reduce_fusion.1
  11.5 7.9 %reshape.184 = f32[16,16,64,64]{3,2,1,0:T(8,128)} reshape(f32[16,16,4096]{2,1,0:T(8,128)} %param.34) | data formatting | bytes 8388608 | tf_op jit(solution)/shard_map/reshape | solution.py:47
  19.7 8.5 %broadcast_multiply_fusion = (f32[16,16,64,64]{3,2,1,0:T(8,128)}, f32[16,16,64]{2,1,0:T(8,128)S(1)}) fusion(f32[16,16,64]{2,1,0:T(8,128)S(1)} %bitcast.46, f32[16,16,64]{2,1,0:T(8,128)S(1)} %multiply_multiply_fusion, f32[16,16,64]{2,1,0:T(8,128)S(1)} %bitcast.47, f32[16,16,64,64]{3,2,1,0:T(8,128)} %reshape.184, f32[16,16]{1,0:T(8,128)S(1)} %get-tuple-element.11), kind=kLoop, calls=%fused_computation.3 | loop fusion | flops 5226496 | bytes 8651776 | tf_op jit(solution)/shard_map/mul | solution.py:48
  28.7 23.2 %all_to_all.24 = bf16[16,16,1024]{2,1,0:T(8,128)(2,1)S(1)} all-to-all(bf16[16,16,1024]{2,1,0:T(8,128)(2,1)S(1)} %stack.2), channel_id=1, replica_groups=mesh['ep'=16,'tp'=2] {'ep'}, dimensions={0} | all-to-all | bytes 1048576 | tf_op jit(solution)/shard_map/all_to_all | solution.py:17
  51.9 0.9 convolution_convert_fusion.2
  52.8 4.0 %all-to-all-start.1 = ((bf16[16,16,128]{2,1,0:T(8,128)(2,1)}), bf16[16,16,128]{2,1,0:T(8,128)(2,1)S(1)}, u32[]{:S(2)}, u32[]{:S(2)}) async-start(bf16[16,16,128]{2,1,0:T(8,128)(2,1)} %bitcast.7), calls=%async_computation.1 | async-start | bytes 131072 | tf_op jit(solution)/shard_map/all_to_all | solution.py:102
  56.8 7.5 %all-to-all-done.1 = bf16[16,16,128]{2,1,0:T(8,128)(2,1)S(1)} async-done(((bf16[16,16,128]{2,1,0:T(8,128)(2,1)}), bf16[16,16,128]{2,1,0:T(8,128)(2,1)S(1)}, u32[]{:S(2)}, u32[]{:S(2)}) %all-to-all-start.1) | async-done | bytes 65568 | tf_op jit(solution)/shard_map/all_to_all | solution.py:102
  65.0 14.6 %all-reduce.2.cloned.1.call-done = bf16[16,2048]{1,0:T(8,128)(2,1)} async-done(((bf16[16,2048]{1,0:T(8,128)(2,1)}), bf16[16,2048]{1,0:T(8,128)(2,1)}) %all-reduce.2.cloned.1.call-update) | async-done | bytes 65552 | tf_op jit(solution)/shard_map/psum | solution.py:105
  79.6 1.0 fusion.21
  80.6 1.6 multiply_convert_fusion
  84.4 54.8 %all-gather.2.cloned.1.call-done = bf16[256,2048]{1,0:T(8,128)(2,1)} async-done(((bf16[16,2048]{1,0:T(8,128)(2,1)}), bf16[256,2048]{1,0:T(8,128)(2,1)}) %all-gather.2.cloned.1.call-update) | async-done | bytes 1048592 | tf_op jit(solution)/shard_map/all_gather | solution.py:113
  139.2 1.6 fusion.36
  140.9 2.8 %gather_fusion = bf16[112,2048]{1,0:T(8,128)(2,1)S(1)} fusion(bf16[256,2048]{1,0:T(8,128)(2,1)} %all-gather.2.cloned.1.call-done, s32[1024]{0:T(1024)S(1)} %pad_clamp_fusion), kind=kCustom, calls=%fused_computation | custom fusion | bytes 917952 | tf_op jit(solution)/shard_map/jit(_take)/gather | solution.py:142
  143.7 1.6 fusion.7
  146.4 1.5 fusion.3
  148.2 3.0 %convolution_convert_fusion = bf16[256,2048]{1,0:T(8,128)(2,1)} fusion(bf16[256,384]{1,0:T(8,128)(2,1)S(1)} %bitcast.50, bf16[256,2048]{1,0:T(8,128)(2,1)} %bitcast.54, bf16[128,2048]{1,0:T(8,128)(2,1)} %param.42), kind=kOutput, calls=%fused_computation.4 | convolution fusion | flops 406323200 | bytes 2818048 | tf_op jit(solution)/shard_map/dot_general | solution.py:161
  151.3 7.3 %reduce-scatter.3.cloned.1.call-done = bf16[128,2048]{1,0:T(8,128)(2,1)} async-done(((bf16[256,2048]{1,0:T(8,128)(2,1)}), bf16[128,2048]{1,0:T(8,128)(2,1)}) %reduce-scatter.3.cloned.1.call-update) | async-done | bytes 524304 | tf_op jit(solution)/shard_map/reduce_scatter | solution.py:160
  158.6 2.2 convert_element_type.106
  160.8 7.9 %mul.284 = f32[16,16,4096]{2,1,0:T(8,128)} reshape(f32[16,16,64,64]{3,2,1,0:T(8,128)} %get-tuple-element.4) | data formatting | bytes 8388608 | tf_op jit(solution)/shard_map/mul | solution.py:48
  168.7 6.6 %multiply_add_fusion = f32[16,16,4096]{2,1,0:T(8,128)} fusion(f32[16,16,4096]{2,1,0:T(8,128)} %mul.284, f32[16,16,4096]{2,1,0:T(8,128)} %param.34, f32[16,16]{1,0:T(8,128)S(1)} %get-tuple-element.11), kind=kLoop, calls=%fused_computation.2 | loop fusion | flops 2097152 | bytes 12583936 | tf_op jit(solution)/shard_map/add | solution.py:49
  175.3 65.8 %reduce-scatter.5.cloned.1.call-done = f32[8,2048]{1,0:T(8,128)} async-done(((f32[128,2048]{1,0:T(8,128)}), f32[8,2048]{1,0:T(8,128)}) %reduce-scatter.5.cloned.1.call-update) | async-done | bytes 65552 | tf_op jit(solution)/shard_map/reduce_scatter | solution.py:166
  241.1 1.5 add_convert_fusion.1
  (90 shorter events, 6.6 us)
Async XLA Ops:
  7.2 138.1 %copy-start = (bf16[1,2048,256]{2,1,0:T(8,128)(2,1)S(1)}, bf16[1,2048,256]{2,1,0:T(8,128)(2,1)}, u32[]{:S(2)}) copy-start(bf16[1,2048,256]{2,1,0:T(8,128)(2,1)} %param.48) | copy-start | bytes 3145732
  11.5 7.9 %copy-start.12 = (bf16[16,16]{1,0:T(8,128)(2,1)S(1)}, bf16[16,16]{1,0:T(8,128)(2,1)}, u32[]{:S(2)}) copy-start(bf16[16,16]{1,0:T(8,128)(2,1)} %param.29) | copy-start | bytes 1540
  11.5 7.9 %copy-start.13 = (f32[16]{0:T(128)S(1)}, f32[16]{0:T(128)}, u32[]{:S(2)}) copy-start(f32[16]{0:T(128)} %param.35) | copy-start | bytes 196
  19.6 8.7 %copy-start.5 = (bf16[16,1024]{1,0:T(8,128)(2,1)S(1)}, bf16[16,1024]{1,0:T(8,128)(2,1)}, u32[]{:S(2)}) copy-start(bf16[16,1024]{1,0:T(8,128)(2,1)} %param.27) | copy-start | bytes 98308
  19.6 8.9 %copy-start.9 = (f32[1024]{0:T(1024)S(1)}, f32[1024]{0:T(1024)}, u32[]{:S(2)}) copy-start(f32[1024]{0:T(1024)} %param.37) | copy-start | bytes 12292
  19.6 32.3 %copy-start.3 = (bf16[1024,128]{1,0:T(8,128)(2,1)S(1)}, bf16[1024,128]{1,0:T(8,128)(2,1)}, u32[]{:S(2)}) copy-start(bf16[1024,128]{1,0:T(8,128)(2,1)} %param.38) | copy-start | bytes 786436
  19.6 45.4 %copy-start.7 = (s32[256,6]{0,1:T(8,128)S(1)}, s32[256,6]{0,1:T(8,128)}, u32[]{:S(2)}) copy-start(s32[256,6]{0,1:T(8,128)} %param.45) | copy-start | bytes 18436
  19.6 60.0 %copy-start.4 = (bf16[16,2048]{1,0:T(8,128)(2,1)S(1)}, bf16[16,2048]{1,0:T(8,128)(2,1)}, u32[]{:S(2)}) copy-start(bf16[16,2048]{1,0:T(8,128)(2,1)} %param.25) | copy-start | bytes 196612
  19.6 60.9 %copy-start.6 = (f32[2048]{0:T(1024)S(1)}, f32[2048]{0:T(1024)}, u32[]{:S(2)}) copy-start(f32[2048]{0:T(1024)} %param.39) | copy-start | bytes 24580
  28.1 55.3 %copy-start.11 = (f32[256,4]{0,1:T(4,128)S(1)}, f32[256,4]{0,1:T(4,128)}, u32[]{:S(2)}) copy-start(f32[256,4]{0,1:T(4,128)} %param.44) | copy-start | bytes 12292
  28.1 55.4 %copy-start.8 = (f32[256,6]{0,1:T(8,128)S(1)}, f32[256,6]{0,1:T(8,128)}, u32[]{:S(2)}) copy-start(f32[256,6]{0,1:T(8,128)} %param.46) | copy-start | bytes 18436
  28.1 56.2 %copy-start.10 = (bf16[2048]{0:T(1024)(128)(2,1)S(1)}, bf16[2048]{0:T(1024)(128)(2,1)}, u32[]{:S(2)}) copy-start(bf16[2048]{0:T(1024)(128)(2,1)} %param.43) | copy-start | bytes 12292
  52.8 11.5 %all-to-all-start.1 = ((bf16[16,16,128]{2,1,0:T(8,128)(2,1)}), bf16[16,16,128]{2,1,0:T(8,128)(2,1)S(1)}, u32[]{:S(2)}, u32[]{:S(2)}) async-start(bf16[16,16,128]{2,1,0:T(8,128)(2,1)} %bitcast.7), calls=%async_computation.1 | async-start | bytes 131072 | tf_op jit(solution)/shard_map/all_to_all | solution.py:102
  56.8 22.8 %all-reduce.2.cloned.1.call-start = ((), (), s32[]{:S(2)}) async-start(), calls=%async_computation.4 | async-start | bytes 131072 | tf_op jit(solution)/shard_map/psum | solution.py:105
  65.0 74.3 %all-gather.2.cloned.1.call-start = ((), (), s32[]{:S(2)}) async-start(), calls=%async_computation.5 | async-start | bytes 1114112 | tf_op jit(solution)/shard_map/all_gather | solution.py:113
  82.2 76.4 %reduce-scatter.3.cloned.1.call-start = ((), (), s32[]{:S(2)}) async-start(), calls=%async_computation.6 | async-start | bytes 1572864 | tf_op jit(solution)/shard_map/reduce_scatter | solution.py:160
  140.8 5.0 %copy-start.1 = (bf16[256,2048]{1,0:T(8,128)(2,1)S(1)}, bf16[256,2048]{1,0:T(8,128)(2,1)}, u32[]{:S(2)}) copy-start(bf16[256,2048]{1,0:T(8,128)(2,1)} %all-gather.2.cloned.1.call-done) | copy-start | bytes 3145732
  140.8 5.1 %copy-start.2 = (bf16[2048,128]{1,0:T(8,128)(2,1)S(1)}, bf16[2048,128]{1,0:T(8,128)(2,1)}, u32[]{:S(2)}) copy-start(bf16[2048,128]{1,0:T(8,128)(2,1)} %param.40) | copy-start | bytes 1572868
  151.2 89.9 %reduce-scatter.5.cloned.1.call-start = ((), (), s32[]{:S(2)}) async-start(), calls=%async_computation.7 | async-start | bytes 1114112 | tf_op jit(solution)/shard_map/reduce_scatter | solution.py:166
Sparse Core Ops, SparseCore 0:
  65.1 14.4 all-reduce.1
  82.9 56.2 all-gather.1
  151.3 7.2 reduce-scatter.2
  161.0 80.0 reduce-scatter.4
